TPU v7x, 512 devices: a whole 4x8x8 slice. The times are simulated.
512 devices in a mesh: ep: 128 (over z, y, core), tp: 4 (over x).
Axes of the slice: x: 4, y: 8, z: 8, core: 2. Of those that a mesh axis runs over, the one named last changes fastest.
Arguments:
- tokens: bfloat16 [16384, 2048], P('ep'), may hold values from -6 to 6
- norm_gain: float32 [2048], replicated, may hold values from 0.1 to 1.9
- routes: int32 [16384, 2], P('ep'), may hold values from 0 to 127, all different within a row; in each aligned block of 128 rows (0 to 127, 128 to 255, ...) at most 3 rows name the same one
- group_prob: float32 [16384], P('ep'), may hold values from 0.2 to 1
- expert_logits: float32 [16384, 2], P('ep'), may hold values from -6 to 6
- gate_weight: bfloat16 [128, 2048, 384], P('ep', None, 'tp'), may hold values from -0.125 to 0.125
- up_weight: bfloat16 [128, 2048, 384], P('ep', None, 'tp'), may hold values from -0.125 to 0.125
- down_matrix: bfloat16 [128, 384, 2048], P('ep', 'tp'), may hold values from -0.3125 to 0.3125
Outputs:
- combined: bfloat16 [16384, 2048], P('ep', 'tp')
Inputs may be any that keep to these rules, and one draw needn't show every extreme that they name: `routes`: each row names 2 different experts. Among the 128 tokens of one index of ep at most 3 rows name one expert, and in every draw some expert is named by exactly 3 of them.
All inputs are finite; a program needn't handle non-finite values.
Results may differ from a plain program's by a relative error of at most 0.013.
Values may be sent and summed in bfloat16 or wider, within the bound.
A program may use at most 64 MiB of HBM per device.

v0:
```python
import jax
import jax.numpy as jnp
from jax import lax
from jax.sharding import PartitionSpec as P


def in_order(parts, dim):
    lengths = list(parts.shape[1:])
    lengths[dim] *= parts.shape[0]
    return jnp.moveaxis(parts, 0, dim).reshape(lengths)


def sent_to_all(shard, axis):
    copies = jnp.broadcast_to(shard, (lax.axis_size(axis), *shard.shape))
    return lax.all_to_all(copies, axis, split_axis=0, concat_axis=0, tiled=True)


def gathered_copies(shard, axis, dim):
    return in_order(sent_to_all(shard, axis), dim)


def hidden_part(buffer, gate_weight, up_weight):
    local_count = gate_weight.shape[0]
    grouped = buffer.reshape(
        buffer.shape[0] // local_count, local_count, buffer.shape[1], buffer.shape[2]
    )
    gate_proj = jnp.einsum(
        "sknd,kdf->sknf", grouped, gate_weight, preferred_element_type=jnp.float32
    )
    up_proj = jnp.einsum("sknd,kdf->sknf", grouped, up_weight, preferred_element_type=jnp.float32)
    hidden_state = (jax.nn.silu(gate_proj) * up_proj).astype(jnp.bfloat16)
    return hidden_state.reshape(buffer.shape[0], buffer.shape[1], hidden_state.shape[3])


def down_blocks(hidden_full, down_cols, block_count):
    local_count = down_cols.shape[0]
    width = hidden_full.shape[2] // block_count
    grouped = hidden_full.reshape(
        hidden_full.shape[0] // local_count, local_count, hidden_full.shape[1], block_count, width
    )
    columns = down_cols.reshape(local_count, block_count, width, down_cols.shape[2])
    block_list = jnp.einsum(
        "sknrf,krfd->sknrd", grouped, columns, preferred_element_type=jnp.float32
    ).astype(jnp.bfloat16)
    summed = jnp.sum(block_list.astype(jnp.float32), 3).astype(jnp.bfloat16)
    return summed.reshape(hidden_full.shape[0], hidden_full.shape[1], down_cols.shape[2])


def body(tokens, norm_gain, routes, group_prob, expert_logits, gate_weight, up_weight, down_matrix):
    tok_rows, model_width = tokens.shape
    top_count = routes.shape[1]
    experts = gate_weight.shape[0] * lax.axis_size("ep")
    capacity = 3 * top_count * tok_rows // (2 * experts)
    block_count = lax.axis_size("tp")
    down_cols = lax.all_to_all(down_matrix, "tp", split_axis=2, concat_axis=1, tiled=True)
    values = tokens.astype(jnp.float32)
    normed = (
        values * lax.rsqrt(jnp.mean(values * values, -1, keepdims=True) + 1e-06) * norm_gain
    ).astype(jnp.bfloat16)
    flat_ids = routes.reshape(-1)
    onehot = (flat_ids[:, None] == jnp.arange(experts, dtype=jnp.int32)[None, :]).astype(jnp.int32)
    earlier = jnp.cumsum(onehot, 0) - onehot
    slot_index = jnp.sum(earlier * onehot, 1)
    target = flat_ids * capacity + slot_index
    owners = jnp.arange(tok_rows * top_count, dtype=jnp.int32) // top_count
    outgoing = (
        jnp.zeros((experts * capacity, model_width), jnp.bfloat16).at[target].set(normed[owners])
    )
    outgoing = outgoing.reshape(experts, capacity, model_width)
    feature_share = model_width // block_count
    my_features = lax.dynamic_slice_in_dim(
        outgoing, lax.axis_index("tp") * feature_share, feature_share, 2
    )
    arrived = lax.all_to_all(my_features, "ep", split_axis=0, concat_axis=0, tiled=True)
    full_rows = gathered_copies(arrived, "tp", 2)
    hidden_state = hidden_part(full_rows, gate_weight, up_weight)
    hidden_full = gathered_copies(hidden_state, "tp", 2)
    summed = down_blocks(hidden_full, down_cols, block_count)
    returned = lax.all_to_all(summed, "ep", split_axis=0, concat_axis=0, tiled=True)
    flat_back = returned.reshape(experts * capacity, returned.shape[2])
    weights = group_prob[:, None] * jax.nn.softmax(expert_logits, axis=-1)
    picked = flat_back[target].reshape(tok_rows, top_count, flat_back.shape[1]).astype(jnp.float32)
    combined = jnp.sum(picked * weights[:, :, None], 1).astype(jnp.bfloat16)
    return combined


def solution(mesh):
    return jax.shard_map(
        body,
        mesh=mesh,
        in_specs=(
            P("ep", None),
            P(),
            P("ep", None),
            P("ep"),
            P("ep", None),
            P("ep", None, "tp"),
            P("ep", None, "tp"),
            P("ep", "tp", None),
        ),
        out_specs=P("ep", "tp"),
        check_vma=False,
    )
```

profile of v0, /device:TPU:1, one launch (start us, length us, event | category | flops | bytes accessed | tf_op | source)
XLA Modules:
  0.0 136.8 jit_solution(1834693873175598776)
XLA Ops:
  0.0 0.0 copy-start
  0.0 0.0 copy-start.1
  0.0 0.0 copy-start.4
  0.0 0.9 copy.34
  0.9 0.1 eq.29
  1.0 0.1 eq.25
  1.2 0.7 broadcast_multiply_fusion
  1.9 0.1 copy.36
  2.0 0.2 fusion.13
  2.3 0.1 copy.33
  2.4 0.1 mul.66
  2.5 1.2 fusion.4
  3.8 0.2 fusion.15
  4.0 0.0 copy-done.1
  4.0 0.0 copy-done.4
  4.0 0.2 fusion.6
  4.2 5.9 %scatter_custom_fusion = bf16[384,2048]{1,0:T(8,128)(2,1)S(1)} fusion(s32[256]{0:T(256)S(1)} %bitcast.72, bf16[128,2048]{1,0:T(8,128)(2,1)S(1)} %fusion.6, s32[1024]{0:T(1024)S(1)} %pad_clamp_fusion.1, bf16[]{:T(256)} %constant.18.clone.1), kind=kCustom, calls=%fused_computation.15 | custom fusion | bytes 1572866 | tf_op jit(solution)/shard_map/scatter | solution.py:67
  10.1 2.3 %reshape.142 = bf16[128,3,2048]{2,1,0:T(4,128)(2,1)} reshape(bf16[384,2048]{1,0:T(8,128)(2,1)S(1)} %scatter_custom_fusion) | data formatting | bytes 3145728 | tf_op jit(solution)/shard_map/reshape | solution.py:69
  12.5 0.0 copy-start.2
  12.5 2.1 %constant_dynamic-slice_fusion = bf16[128,3,512]{2,1,0:T(4,128)(2,1)} fusion(bf16[128,3,2048]{2,1,0:T(4,128)(2,1)} %reshape.142, s32[]{:T(128)S(6)} %select_n.39), kind=kLoop, calls=%fused_computation.46 | loop fusion | bytes 786436 | tf_op jit(solution)/shard_map/dynamic_slice | solution.py:71
  14.5 18.4 %all-to-all-start.1 = ((bf16[128,3,512]{2,1,0:T(4,128)(2,1)}), bf16[128,3,512]{2,1,0:T(4,128)(2,1)S(1)}, u32[]{:S(2)}, u32[]{:S(2)}) async-start(bf16[128,3,512]{2,1,0:T(4,128)(2,1)} %constant_dynamic-slice_fusion), calls=%async_computation.1 | async-start | bytes 1048576 | tf_op jit(solution)/shard_map/all_to_all | solution.py:74
  33.0 0.0 copy-done.2
  33.0 0.8 copy.28
  33.7 0.5 broadcast.137
  34.2 11.5 %reduce.4 = bf16[2048,96]{1,0:T(8,128)(2,1)S(1)} reduce(bf16[2048,1,96]{2,1,0:T(2,128)(2,1)S(1)} %bitcast.65, bf16[]{:T(256)} %broadcast.137), dimensions={1}, to_apply=%bitcast.53.reduce_sub_computation | reduce | bytes 786434
  45.8 1.6 %reshape.182 = bf16[4,2,24576]{2,1,0:T(2,128)(2,1)} reshape(bf16[2048,96]{1,0:T(8,128)(2,1)S(1)} %reduce.4) | data formatting | bytes 786432
  47.3 6.2 %all-to-all-done.1 = bf16[128,3,512]{2,1,0:T(4,128)(2,1)S(1)} async-done(((bf16[128,3,512]{2,1,0:T(4,128)(2,1)}), bf16[128,3,512]{2,1,0:T(4,128)(2,1)S(1)}, u32[]{:S(2)}, u32[]{:S(2)}) %all-to-all-start.1) | async-done | bytes 393248 | tf_op jit(solution)/shard_map/all_to_all | solution.py:74
  53.5 4.0 %all-to-all-start = ((bf16[4,2,24576]{2,1,0:T(2,128)(2,1)}), bf16[4,2,24576]{2,1,0:T(2,128)(2,1)S(1)}, u32[]{:S(2)}, u32[]{:S(2)}) async-start(bf16[4,2,24576]{2,1,0:T(2,128)(2,1)} %reshape.182), calls=%async_computation | async-start | bytes 786432 | tf_op jit(solution)/shard_map/all_to_all | solution.py:55
  57.5 0.1 copy.38
  57.6 8.1 %all-to-all-done = bf16[4,2,24576]{2,1,0:T(2,128)(2,1)S(1)} async-done(((bf16[4,2,24576]{2,1,0:T(2,128)(2,1)}), bf16[4,2,24576]{2,1,0:T(2,128)(2,1)S(1)}, u32[]{:S(2)}, u32[]{:S(2)}) %all-to-all-start) | async-done | bytes 393248 | tf_op jit(solution)/shard_map/all_to_all | solution.py:55
  65.7 1.3 broadcast_in_dim.7
  67.0 3.6 %all-to-all-start.2 = ((bf16[4,128,3,512]{3,1,2,0:T(8,128)(2,1)}), bf16[4,128,3,512]{3,1,2,0:T(8,128)(2,1)S(1)}, u32[]{:S(2)}, u32[]{:S(2)}) async-start(bf16[4,128,3,512]{3,1,2,0:T(8,128)(2,1)} %broadcast_in_dim.7), calls=%async_computation.2 | async-start | bytes 3145728 | tf_op jit(solution)/shard_map/all_to_all | solution.py:15
  70.5 0.8 reshape.183
  71.3 19.1 %all-to-all-done.2 = bf16[4,128,3,512]{3,1,2,0:T(8,128)(2,1)S(1)} async-done(((bf16[4,128,3,512]{3,1,2,0:T(8,128)(2,1)}), bf16[4,128,3,512]{3,1,2,0:T(8,128)(2,1)S(1)}, u32[]{:S(2)}, u32[]{:S(2)}) %all-to-all-start.2) | async-done | bytes 1572896 | tf_op jit(solution)/shard_map/all_to_all | solution.py:15
  90.4 0.2 copy.43
  90.6 0.0 copy-start.6
  90.6 0.0 copy-done
  90.6 0.6 convolution_bitcast_fusion.1
  91.2 0.4 copy-done.6
  91.6 0.6 fusion.3
  92.2 0.7 broadcast_in_dim.8
  93.0 3.5 %all-to-all-start.3 = ((bf16[4,128,3,96]{1,3,2,0:T(8,128)(2,1)}), bf16[4,128,3,96]{1,3,2,0:T(8,128)(2,1)S(1)}, u32[]{:S(2)}, u32[]{:S(2)}) async-start(bf16[4,128,3,96]{1,3,2,0:T(8,128)(2,1)} %broadcast_in_dim.8), calls=%async_computation.3 | async-start | bytes 589824 | tf_op jit(solution)/shard_map/all_to_all | solution.py:15
  96.4 1.1 fusion.19
  97.5 0.1 copy.29
  97.6 0.1 copy.30
  97.8 0.1 copy.31
  97.9 0.1 copy.32
  98.1 4.0 %all-to-all-done.3 = bf16[4,128,3,96]{1,3,2,0:T(8,128)(2,1)S(1)} async-done(((bf16[4,128,3,96]{1,3,2,0:T(8,128)(2,1)}), bf16[4,128,3,96]{1,3,2,0:T(8,128)(2,1)S(1)}, u32[]{:S(2)}, u32[]{:S(2)}) %all-to-all-start.3) | async-done | bytes 294944 | tf_op jit(solution)/shard_map/all_to_all | solution.py:15
  102.1 0.0 copy-start.3
  102.1 0.0 copy-start.5
  102.1 0.6 fusion
  102.7 1.2 copy.40
  103.9 9.1 %all-to-all-start.4 = ((bf16[128,3,512]{2,1,0:T(4,128)(2,1)}), bf16[128,3,512]{2,1,0:T(4,128)(2,1)S(1)}, u32[]{:S(2)}, u32[]{:S(2)}) async-start(bf16[128,3,512]{2,1,0:T(4,128)(2,1)} %copy.40), calls=%async_computation.4 | async-start | bytes 1048576 | tf_op jit(solution)/shard_map/all_to_all | solution.py:79
  113.0 0.0 copy-done.3
  113.1 0.0 copy-done.5
  113.1 0.1 copy.41
  113.2 20.4 %all-to-all-done.4 = bf16[128,3,512]{2,1,0:T(4,128)(2,1)S(1)} async-done(((bf16[128,3,512]{2,1,0:T(4,128)(2,1)}), bf16[128,3,512]{2,1,0:T(4,128)(2,1)S(1)}, u32[]{:S(2)}, u32[]{:S(2)}) %all-to-all-start.4) | async-done | bytes 393248 | tf_op jit(solution)/shard_map/all_to_all | solution.py:79
  133.6 0.3 reshape.147
  133.9 1.2 gather_fusion
  135.1 0.3 reshape.148
  135.4 1.4 multiply_reduce_fusion
  (15 shorter events, 0.2 us)
Async XLA Ops:
  0.0 90.6 %copy-start = (bf16[1,2048,96]{1,2,0:T(8,128)(2,1)S(1)}, bf16[1,2048,96]{1,2,0:T(8,128)(2,1)}, u32[]{:S(2)}) copy-start(bf16[1,2048,96]{1,2,0:T(8,128)(2,1)} %param.13) | copy-start | bytes 1179652
  0.0 4.0 %copy-start.1 = (bf16[128,2048]{1,0:T(8,128)(2,1)S(1)}, bf16[128,2048]{1,0:T(8,128)(2,1)}, u32[]{:S(2)}) copy-start(bf16[128,2048]{1,0:T(8,128)(2,1)} %param.8) | copy-start | bytes 1572868
  0.0 4.0 %copy-start.4 = (f32[2048]{0:T(1024)S(1)}, f32[2048]{0:T(1024)}, u32[]{:S(2)}) copy-start(f32[2048]{0:T(1024)} %param.9) | copy-start | bytes 24580
  12.5 20.5 %copy-start.2 = (bf16[1,96,2048]{2,1,0:T(8,128)(2,1)S(1)}, bf16[1,96,2048]{2,1,0:T(8,128)(2,1)}, u32[]{:S(2)}) copy-start(bf16[1,96,2048]{2,1,0:T(8,128)(2,1)} %param.15) | copy-start | bytes 1179652
  14.5 39.0 %all-to-all-start.1 = ((bf16[128,3,512]{2,1,0:T(4,128)(2,1)}), bf16[128,3,512]{2,1,0:T(4,128)(2,1)S(1)}, u32[]{:S(2)}, u32[]{:S(2)}) async-start(bf16[128,3,512]{2,1,0:T(4,128)(2,1)} %constant_dynamic-slice_fusion), calls=%async_computation.1 | async-start | bytes 1048576 | tf_op jit(solution)/shard_map/all_to_all | solution.py:74
  53.5 12.2 %all-to-all-start = ((bf16[4,2,24576]{2,1,0:T(2,128)(2,1)}), bf16[4,2,24576]{2,1,0:T(2,128)(2,1)S(1)}, u32[]{:S(2)}, u32[]{:S(2)}) async-start(bf16[4,2,24576]{2,1,0:T(2,128)(2,1)} %reshape.182), calls=%async_computation | async-start | bytes 786432 | tf_op jit(solution)/shard_map/all_to_all | solution.py:55
  67.0 23.5 %all-to-all-start.2 = ((bf16[4,128,3,512]{3,1,2,0:T(8,128)(2,1)}), bf16[4,128,3,512]{3,1,2,0:T(8,128)(2,1)S(1)}, u32[]{:S(2)}, u32[]{:S(2)}) async-start(bf16[4,128,3,512]{3,1,2,0:T(8,128)(2,1)} %broadcast_in_dim.7), calls=%async_computation.2 | async-start | bytes 3145728 | tf_op jit(solution)/shard_map/all_to_all | solution.py:15
  90.6 1.0 copy-start.6
  93.0 9.1 %all-to-all-start.3 = ((bf16[4,128,3,96]{1,3,2,0:T(8,128)(2,1)}), bf16[4,128,3,96]{1,3,2,0:T(8,128)(2,1)S(1)}, u32[]{:S(2)}, u32[]{:S(2)}) async-start(bf16[4,128,3,96]{1,3,2,0:T(8,128)(2,1)} %broadcast_in_dim.8), calls=%async_computation.3 | async-start | bytes 589824 | tf_op jit(solution)/shard_map/all_to_all | solution.py:15
  102.1 11.0 %copy-start.3 = (f32[128,2]{0,1:T(2,128)S(1)}, f32[128,2]{0,1:T(2,128)}, u32[]{:S(2)}) copy-start(f32[128,2]{0,1:T(2,128)} %param.12) | copy-start | bytes 3076
  102.1 11.0 %copy-start.5 = (f32[128]{0:T(128)S(1)}, f32[128]{0:T(128)}, u32[]{:S(2)}) copy-start(f32[128]{0:T(128)} %param.11) | copy-start | bytes 1540
  103.9 29.7 %all-to-all-start.4 = ((bf16[128,3,512]{2,1,0:T(4,128)(2,1)}), bf16[128,3,512]{2,1,0:T(4,128)(2,1)S(1)}, u32[]{:S(2)}, u32[]{:S(2)}) async-start(bf16[128,3,512]{2,1,0:T(4,128)(2,1)} %copy.40), calls=%async_computation.4 | async-start | bytes 1048576 | tf_op jit(solution)/shard_map/all_to_all | solution.py:79
where the time goes:
time: 137 us
  waiting for transfers between devices  57.7 us (42%)
  starting transfers between devices  38.6 us (28%)
  local copies, waits for them, and re-layouts  22.9 us (17%)
  other arithmetic  15.6 us (11%)
  matrix products  1.82 us (1%)
    all_to_all x2, waiting for transfers between devices, sent_to_all(): return lax.all_to_all(copies, axis, split_axis=0, concat_axis=0, tiled=True)  23.1 us
    all_to_all x1, waiting for transfers between devices, body(): lax.all_to_all(summed, 'ep', split_axis=0, concat_axis=0, tiled=True)  20.4 us
    all_to_all x1, starting transfers between devices, body(): lax.all_to_all(my_features, 'ep', split_axis=0, concat_axis=0, tiled=True)  18.4 us
    unnamed x1, other arithmetic  11.5 us
    all_to_all x1, starting transfers between devices, body(): lax.all_to_all(summed, 'ep', split_axis=0, concat_axis=0, tiled=True)  9.14 us
    all_to_all x1, waiting for transfers between devices, body(): lax.all_to_all(down_matrix, 'tp', split_axis=2, concat_axis=1, tiled=True)  8.05 us
    all_to_all x2, starting transfers between devices, sent_to_all(): return lax.all_to_all(copies, axis, split_axis=0, concat_axis=0, tiled=True)  7.01 us
    all_to_all x1, waiting for transfers between devices, body(): lax.all_to_all(my_features, 'ep', split_axis=0, concat_axis=0, tiled=True)  6.16 us
  transfers between devices with their start and end apart: 5, of which 5 were waited for; matrix products, arithmetic and copies ran while one was open for 12% of the time, Pallas kernels for 0%

commit v1 on v0

--- a/solution.py
+++ b/solution.py
@@ -1,7 +1,40 @@
+import functools
 import jax
 import jax.numpy as jnp
 from jax import lax
 from jax.sharding import PartitionSpec as P
+
+
+def leaf_render(u, along_dim, my_data):
+    ready = u.shape
+    main = u.reshape(
+        *ready[:along_dim], my_data, ready[along_dim] // my_data, *ready[along_dim + 1 :]
+    )
+    return jnp.moveaxis(main, along_dim, 0)
+
+
+def _check_boxes(content, out_dim):
+    w_next = list(content.shape[1:])
+    w_next[out_dim] *= content.shape[0]
+    return jnp.moveaxis(content, 0, out_dim).reshape(w_next)
+
+
+def launch_teams(z, field_in, across, frame):
+    newest, arr_now = (lax.axis_size(across), lax.axis_index(across))
+    field_out = leaf_render(z, field_in, newest)
+    fields = [field_out[arr_now]]
+    for no in [*range(1, newest)]:
+        work_now = field_out[(arr_now + no) % newest]
+        fields.append(
+            lax.ppermute(
+                work_now, axis_name=across, perm=[(k, (k + no) % newest) for k in range(newest)]
+            )
+        )
+    field_out = jnp.stack(fields, 0)[(arr_now - jnp.arange(newest)) % newest]
+    return _check_boxes(field_out, frame)
+
+
+row_deliver = functools.partial(launch_teams, field_in=2, across="tp", frame=1)
 
 
 def in_order(parts, dim):
@@ -52,7 +85,7 @@
     experts = gate_weight.shape[0] * lax.axis_size("ep")
     capacity = 3 * top_count * tok_rows // (2 * experts)
     block_count = lax.axis_size("tp")
-    down_cols = lax.all_to_all(down_matrix, "tp", split_axis=2, concat_axis=1, tiled=True)
+    down_cols = row_deliver(down_matrix)
     values = tokens.astype(jnp.float32)
     normed = (
         values * lax.rsqrt(jnp.mean(values * values, -1, keepdims=True) + 1e-06) * norm_gain

time: 137 us -> 124 us (0.905)
  blocking collectives: 0 us -> 38.8 us
  waiting for transfers between devices: 57.7 us -> 33.9 us
  other arithmetic: 15.6 us -> 3.02 us
  starting transfers between devices: 38.6 us -> 26.7 us
  local copies, waits for them, and re-layouts: 22.9 us -> 18.6 us
    all_to_all x0 -> x1, blocking collectives: none -> 38.8 us  [body(): lax.all_to_all(my_features, 'ep', split_axis=0, concat_axis=0, tiled=True)]
    all_to_all x2 -> x0, starting transfers between devices: 22.4 us -> none  [the longest x1 18.4 us: body(): lax.all_to_all(my_features, 'ep', split_axis=0, concat_axis=0, tiled=True)]
    all_to_all x2 -> x0, waiting for transfers between devices: 14.2 us -> none  [the longest x1 8.05 us: body(): lax.all_to_all(down_matrix, 'tp', split_axis=2, concat_axis=1, tiled=True)]
    unnamed x1 -> x0, other arithmetic: 11.5 us -> none
    ppermute x0 -> x3, starting transfers between devices: none -> 10.9 us  [launch_teams(): lax.ppermute(work_now, axis_name=across, perm=[(k, (k + no) % newest) for...]
    all_to_all x2, waiting for transfers between devices: 23.1 us -> 13.6 us  [sent_to_all(): return lax.all_to_all(copies, axis, split_axis=0, concat_axis=0, tiled=True)]
    unnamed x20, local copies, waits for them, and re-layouts: 4.89 us -> 1.35 us
  transfers between devices with their start and end apart: 5 -> 6, of which waited for: 5 -> 3; matrix products, arithmetic and copies ran while one was open for 12% -> 3% of each run, Pallas kernels for 0% -> 0%
where the time goes in v1:
time: 124 us; the launch traced here: 123 us
  blocking collectives  38.8 us (31%)
  waiting for transfers between devices  33.9 us (27%)
  starting transfers between devices  26.7 us (22%)
  local copies, waits for them, and re-layouts  18.6 us (15%)
  other arithmetic  3.02 us (2%)
  matrix products  1.81 us (1%)
    all_to_all x1, blocking collectives, body(): lax.all_to_all(my_features, 'ep', split_axis=0, concat_axis=0, tiled=True)  38.8 us
    all_to_all x1, waiting for transfers between devices, body(): lax.all_to_all(summed, 'ep', split_axis=0, concat_axis=0, tiled=True)  20.4 us
    all_to_all x2, waiting for transfers between devices, sent_to_all(): return lax.all_to_all(copies, axis, split_axis=0, concat_axis=0, tiled=True)  13.6 us
    ppermute x3, starting transfers between devices, launch_teams(): lax.ppermute(work_now, axis_name=across, perm=[(k, (k + no) % newest) for...  10.9 us
    all_to_all x1, starting transfers between devices, body(): lax.all_to_all(summed, 'ep', split_axis=0, concat_axis=0, tiled=True)  8.17 us
    all_to_all x2, starting transfers between devices, sent_to_all(): return lax.all_to_all(copies, axis, split_axis=0, concat_axis=0, tiled=True)  7.59 us
    scatter x1, local copies, waits for them, and re-layouts, body(): jnp.zeros((experts * capacity, model_width), jnp.bfloat16).at[target]  5.92 us
  transfers between devices with their start and end apart: 6, of which 3 were waited for; matrix products, arithmetic and copies ran while one was open for 3% of the time, Pallas kernels for 0%

profile of v1, /device:TPU:1, one launch (start us, length us, event | category | flops | bytes accessed | tf_op | source)
XLA Modules:
  0.0 123.2 jit_solution(9351460658881410709)
XLA Ops:
  0.0 0.0 copy-start
  0.0 0.0 copy-start.1
  0.0 0.0 copy-start.4
  0.0 0.9 copy.34
  0.9 0.1 eq.35
  1.0 0.1 eq.31
  1.2 0.7 broadcast_multiply_fusion
  1.8 0.1 copy.36
  2.0 0.2 fusion.14
  2.3 0.1 copy.33
  2.4 0.1 mul.66
  2.5 0.2 fusion.16
  2.7 0.0 copy-done.1
  2.7 0.2 fusion.4
  2.9 0.0 copy-done.4
  2.9 0.2 fusion.6
  3.1 5.9 %scatter_custom_fusion = bf16[384,2048]{1,0:T(8,128)(2,1)S(1)} fusion(s32[256]{0:T(256)S(1)} %bitcast.92, bf16[128,2048]{1,0:T(8,128)(2,1)S(1)} %fusion.6, s32[1024]{0:T(1024)S(1)} %pad_clamp_fusion.1, bf16[]{:T(256)} %constant.73.clone.1), kind=kCustom, calls=%fused_computation.16 | custom fusion | bytes 1572866 | tf_op jit(solution)/shard_map/scatter | solution.py:100
  9.1 2.3 %reshape.201 = bf16[128,3,2048]{2,1,0:T(4,128)(2,1)} reshape(bf16[384,2048]{1,0:T(8,128)(2,1)S(1)} %scatter_custom_fusion) | data formatting | bytes 3145728 | tf_op jit(solution)/shard_map/reshape | solution.py:102
  11.4 1.2 constant_dynamic-slice_fusion
  12.6 38.8 %all_to_all.20 = bf16[128,3,512]{2,1,0:T(4,128)(2,1)S(1)} all-to-all(bf16[128,3,512]{2,1,0:T(4,128)(2,1)S(1)} %constant_dynamic-slice_fusion), channel_id=1, replica_groups=mesh['ep'=128,'tp'=4] {'ep'}, dimensions={0} | all-to-all | bytes 786432 | tf_op jit(solution)/shard_map/all_to_all | solution.py:107
  51.4 0.1 copy.38
  51.5 1.3 %broadcast_in_dim.7 = bf16[4,128,3,512]{3,1,2,0:T(8,128)(2,1)} broadcast(bf16[128,3,512]{2,0,1:T(8,128)(2,1)S(1)} %copy.38), dimensions={1,2,3} | broadcast | bytes 1966080 | tf_op jit(solution)/shard_map/broadcast_in_dim | solution.py:47
  52.8 0.0 copy-start.2
  52.8 4.1 %all-to-all-start.1 = ((bf16[4,128,3,512]{3,1,2,0:T(8,128)(2,1)}), bf16[4,128,3,512]{3,1,2,0:T(8,128)(2,1)S(1)}, u32[]{:S(2)}, u32[]{:S(2)}) async-start(bf16[4,128,3,512]{3,1,2,0:T(8,128)(2,1)} %broadcast_in_dim.7), calls=%async_computation.1 | async-start | bytes 3145728 | tf_op jit(solution)/shard_map/all_to_all | solution.py:48
  56.9 0.0 copy-done.2
  56.9 0.3 reshape.198
  57.2 0.8 constant_dynamic-slice_fusion.4
  58.1 3.4 %collective-permute-start = (bf16[1,96,512]{2,1,0:T(8,128)(2,1)S(1)}, bf16[1,96,512]{2,1,0:T(8,128)(2,1)S(1)}, u32[]{:S(2)}, u32[]{:S(2)}) collective-permute-start(bf16[1,96,512]{2,1,0:T(8,128)(2,1)S(1)} %bitcast.87), channel_id=1, source_target_pairs={{0,1},{1,2},{2,3},{3,0},{4,5},{5,6},{6,7},{7,4},{8,9},{9,10},{10,1... | collective-permute-start | bytes 294920 | tf_op jit(solution)/shard_map/ppermute | solution.py:29
  61.5 4.3 %collective-permute-start.1 = (bf16[1,96,512]{2,1,0:T(8,128)(2,1)S(1)}, bf16[1,96,512]{2,1,0:T(8,128)(2,1)S(1)}, u32[]{:S(2)}, u32[]{:S(2)}) collective-permute-start(bf16[1,96,512]{2,1,0:T(8,128)(2,1)S(1)} %bitcast.88), channel_id=1, source_target_pairs={{0,2},{1,3},{2,0},{3,1},{4,6},{5,7},{6,4},{7,5},{8,10},{9,11},{10,... | collective-permute-start | bytes 294920 | tf_op jit(solution)/shard_map/ppermute | solution.py:29
  65.8 3.3 %collective-permute-start.2 = (bf16[1,96,512]{2,1,0:T(8,128)(2,1)S(1)}, bf16[1,96,512]{2,1,0:T(8,128)(2,1)S(1)}, u32[]{:S(2)}, u32[]{:S(2)}) collective-permute-start(bf16[1,96,512]{2,1,0:T(8,128)(2,1)S(1)} %bitcast.89), channel_id=1, source_target_pairs={{0,3},{1,0},{2,1},{3,2},{4,7},{5,4},{6,5},{7,6},{8,11},{9,8},{10,9... | collective-permute-start | bytes 294920 | tf_op jit(solution)/shard_map/ppermute | solution.py:29
  69.2 8.6 %all-to-all-done.1 = bf16[4,128,3,512]{3,1,2,0:T(8,128)(2,1)S(1)} async-done(((bf16[4,128,3,512]{3,1,2,0:T(8,128)(2,1)}), bf16[4,128,3,512]{3,1,2,0:T(8,128)(2,1)S(1)}, u32[]{:S(2)}, u32[]{:S(2)}) %all-to-all-start.1) | async-done | bytes 1572896 | tf_op jit(solution)/shard_map/all_to_all | solution.py:48
  77.8 0.2 copy.47
  77.9 0.0 copy-start.6
  78.0 0.0 copy-done
  78.0 0.6 convolution_bitcast_fusion.1
  78.6 0.4 copy-done.6
  79.0 0.6 fusion.3
  79.5 0.7 broadcast_in_dim.8
  80.3 3.5 %all-to-all-start.2 = ((bf16[4,128,3,96]{1,3,2,0:T(8,128)(2,1)}), bf16[4,128,3,96]{1,3,2,0:T(8,128)(2,1)S(1)}, u32[]{:S(2)}, u32[]{:S(2)}) async-start(bf16[4,128,3,96]{1,3,2,0:T(8,128)(2,1)} %broadcast_in_dim.8), calls=%async_computation.2 | async-start | bytes 589824 | tf_op jit(solution)/shard_map/all_to_all | solution.py:48
  83.8 0.0 collective-permute-done
  83.8 0.0 collective-permute-done.1
  83.8 0.0 collective-permute-done.2
  83.8 0.1 maximum_bitcast_fusion
  83.9 0.6 gather_fusion
  84.4 0.0 copy-start.3
  84.5 0.0 copy-start.5
  84.5 5.0 %all-to-all-done.2 = bf16[4,128,3,96]{1,3,2,0:T(8,128)(2,1)S(1)} async-done(((bf16[4,128,3,96]{1,3,2,0:T(8,128)(2,1)}), bf16[4,128,3,96]{1,3,2,0:T(8,128)(2,1)S(1)}, u32[]{:S(2)}, u32[]{:S(2)}) %all-to-all-start.2) | async-done | bytes 294944 | tf_op jit(solution)/shard_map/all_to_all | solution.py:48
  89.4 0.6 fusion
  90.0 1.2 copy.40
  91.2 8.2 %all-to-all-start.3 = ((bf16[128,3,512]{2,1,0:T(4,128)(2,1)}), bf16[128,3,512]{2,1,0:T(4,128)(2,1)S(1)}, u32[]{:S(2)}, u32[]{:S(2)}) async-start(bf16[128,3,512]{2,1,0:T(4,128)(2,1)} %copy.40), calls=%async_computation.3 | async-start | bytes 1048576 | tf_op jit(solution)/shard_map/all_to_all | solution.py:112
  99.4 0.0 copy-done.3
  99.5 0.0 copy-done.5
  99.5 0.1 copy.41
  99.6 20.4 %all-to-all-done.3 = bf16[128,3,512]{2,1,0:T(4,128)(2,1)S(1)} async-done(((bf16[128,3,512]{2,1,0:T(4,128)(2,1)}), bf16[128,3,512]{2,1,0:T(4,128)(2,1)S(1)}, u32[]{:S(2)}, u32[]{:S(2)}) %all-to-all-start.3) | async-done | bytes 393248 | tf_op jit(solution)/shard_map/all_to_all | solution.py:112
  120.0 0.3 reshape.206
  120.3 1.2 gather_fusion.1
  121.5 0.3 reshape.207
  121.8 1.4 %multiply_reduce_fusion = bf16[128,512]{1,0:T(8,128)(2,1)} fusion(f32[128,2,512]{2,1,0:T(2,128)S(1)} %reshape.207, f32[128,2]{1,0:T(8,128)S(1)} %copy.41), kind=kLoop, calls=%fused_computation.19 | loop fusion | flops 196608 | bytes 656384 | tf_op jit(solution)/shard_map/reduce_sum | solution.py:116
  (19 shorter events, 0.2 us)
Async XLA Ops:
  0.0 78.0 %copy-start = (bf16[1,2048,96]{1,2,0:T(8,128)(2,1)S(1)}, bf16[1,2048,96]{1,2,0:T(8,128)(2,1)}, u32[]{:S(2)}) copy-start(bf16[1,2048,96]{1,2,0:T(8,128)(2,1)} %param.13) | copy-start | bytes 1179652
  0.0 2.7 %copy-start.1 = (bf16[128,2048]{1,0:T(8,128)(2,1)S(1)}, bf16[128,2048]{1,0:T(8,128)(2,1)}, u32[]{:S(2)}) copy-start(bf16[128,2048]{1,0:T(8,128)(2,1)} %param.8) | copy-start | bytes 1572868
  0.0 2.9 %copy-start.4 = (f32[2048]{0:T(1024)S(1)}, f32[2048]{0:T(1024)}, u32[]{:S(2)}) copy-start(f32[2048]{0:T(1024)} %param.9) | copy-start | bytes 24580
  52.8 4.1 %copy-start.2 = (bf16[1,96,2048]{2,1,0:T(8,128)(2,1)S(1)}, bf16[1,96,2048]{2,1,0:T(8,128)(2,1)}, u32[]{:S(2)}) copy-start(bf16[1,96,2048]{2,1,0:T(8,128)(2,1)} %param.15) | copy-start | bytes 1179652
  52.8 25.0 %all-to-all-start.1 = ((bf16[4,128,3,512]{3,1,2,0:T(8,128)(2,1)}), bf16[4,128,3,512]{3,1,2,0:T(8,128)(2,1)S(1)}, u32[]{:S(2)}, u32[]{:S(2)}) async-start(bf16[4,128,3,512]{3,1,2,0:T(8,128)(2,1)} %broadcast_in_dim.7), calls=%async_computation.1 | async-start | bytes 3145728 | tf_op jit(solution)/shard_map/all_to_all | solution.py:48
  58.1 25.7 %collective-permute-start = (bf16[1,96,512]{2,1,0:T(8,128)(2,1)S(1)}, bf16[1,96,512]{2,1,0:T(8,128)(2,1)S(1)}, u32[]{:S(2)}, u32[]{:S(2)}) collective-permute-start(bf16[1,96,512]{2,1,0:T(8,128)(2,1)S(1)} %bitcast.87), channel_id=1, source_target_pairs={{0,1},{1,2},{2,3},{3,0},{4,5},{5,6},{6,7},{7,4},{8,9},{9,10},{10,1... | collective-permute-start | bytes 294920 | tf_op jit(solution)/shard_map/ppermute | solution.py:29
  61.5 22.3 %collective-permute-start.1 = (bf16[1,96,512]{2,1,0:T(8,128)(2,1)S(1)}, bf16[1,96,512]{2,1,0:T(8,128)(2,1)S(1)}, u32[]{:S(2)}, u32[]{:S(2)}) collective-permute-start(bf16[1,96,512]{2,1,0:T(8,128)(2,1)S(1)} %bitcast.88), channel_id=1, source_target_pairs={{0,2},{1,3},{2,0},{3,1},{4,6},{5,7},{6,4},{7,5},{8,10},{9,11},{10,... | collective-permute-start | bytes 294920 | tf_op jit(solution)/shard_map/ppermute | solution.py:29
  65.8 18.0 %collective-permute-start.2 = (bf16[1,96,512]{2,1,0:T(8,128)(2,1)S(1)}, bf16[1,96,512]{2,1,0:T(8,128)(2,1)S(1)}, u32[]{:S(2)}, u32[]{:S(2)}) collective-permute-start(bf16[1,96,512]{2,1,0:T(8,128)(2,1)S(1)} %bitcast.89), channel_id=1, source_target_pairs={{0,3},{1,0},{2,1},{3,2},{4,7},{5,4},{6,5},{7,6},{8,11},{9,8},{10,9... | collective-permute-start | bytes 294920 | tf_op jit(solution)/shard_map/ppermute | solution.py:29
  77.9 1.0 copy-start.6
  80.3 9.1 %all-to-all-start.2 = ((bf16[4,128,3,96]{1,3,2,0:T(8,128)(2,1)}), bf16[4,128,3,96]{1,3,2,0:T(8,128)(2,1)S(1)}, u32[]{:S(2)}, u32[]{:S(2)}) async-start(bf16[4,128,3,96]{1,3,2,0:T(8,128)(2,1)} %broadcast_in_dim.8), calls=%async_computation.2 | async-start | bytes 589824 | tf_op jit(solution)/shard_map/all_to_all | solution.py:48
  84.4 15.0 %copy-start.3 = (f32[128,2]{0,1:T(2,128)S(1)}, f32[128,2]{0,1:T(2,128)}, u32[]{:S(2)}) copy-start(f32[128,2]{0,1:T(2,128)} %param.12) | copy-start | bytes 3076
  84.5 15.0 %copy-start.5 = (f32[128]{0:T(128)S(1)}, f32[128]{0:T(128)}, u32[]{:S(2)}) copy-start(f32[128]{0:T(128)} %param.11) | copy-start | bytes 1540
  91.2 28.7 %all-to-all-start.3 = ((bf16[128,3,512]{2,1,0:T(4,128)(2,1)}), bf16[128,3,512]{2,1,0:T(4,128)(2,1)S(1)}, u32[]{:S(2)}, u32[]{:S(2)}) async-start(bf16[128,3,512]{2,1,0:T(4,128)(2,1)} %copy.40), calls=%async_computation.3 | async-start | bytes 1048576 | tf_op jit(solution)/shard_map/all_to_all | solution.py:112
